TPU v7x, 256 devices: a 4x2x16 block of a 4x16x16 slice. The times are simulated.
256 devices in a mesh: grp: 2 (over y), kv: 16 (over z), tp: 8 (over x, core).
Axes of the slice: x: 4, y: 2, z: 16, core: 2. Of those that a mesh axis runs over, the one named last changes fastest.
The devices are a block of a 4x16x16 slice.
Arguments:
- stream: bfloat16 [256, 2048], P('grp', ('kv', 'tp')), parts along dimension 0, may hold values from -72 to 72
- lengths: int32 [256], P(('grp', 'kv')), parts along dimension 0, may hold values from 1 to 8, 384 in all
- delta_state: float32 [256, 32, 128, 128], P(('grp', 'kv'), 'tp'), parts along dimension 0, may hold values from -0.6 to 0.6
- q_hist: bfloat16 [256, 3, 2048], P(('grp', 'kv'), None, 'tp'), parts along dimension 0, may hold values from -6 to 6
- k_hist: bfloat16 [256, 3, 2048], P(('grp', 'kv'), None, 'tp'), parts along dimension 0, may hold values from -6 to 6
- v_hist: bfloat16 [256, 3, 4096], P(('grp', 'kv'), None, 'tp'), parts along dimension 0, may hold values from -6 to 6
- norm_gain: bfloat16 [2048], replicated, may hold values from 0.099609375 to 1.8984375
- w_query: bfloat16 [2048, 2048], P('kv', 'tp'), may hold values from -0.125 to 0.125
- w_key: bfloat16 [2048, 2048], P('kv', 'tp'), may hold values from -0.125 to 0.125
- w_value: bfloat16 [2048, 4096], P('kv', 'tp'), may hold values from -0.125 to 0.125
- w_gate: bfloat16 [2048, 4096], P('kv', 'tp'), may hold values from -0.125 to 0.125
- w_beta: bfloat16 [2048, 32], replicated, may hold values from -0.125 to 0.125
- w_decay: bfloat16 [2048, 32], replicated, may hold values from -0.125 to 0.125
- conv_query: bfloat16 [4, 2048], replicated, may hold values from -3 to 3
- conv_key: bfloat16 [4, 2048], replicated, may hold values from -3 to 3
- conv_value: bfloat16 [4, 4096], replicated, may hold values from -3 to 3
- decay_log: float32 [32], replicated, may hold values from 0 to 2.77
- time_bias: float32 [32], replicated, may hold values from -4 to 0
- out_gain: bfloat16 [128], replicated, may hold values from 0.099609375 to 1.8984375
- w_out: bfloat16 [4096, 2048], P('tp', 'kv'), may hold values from -0.09375 to 0.09375
- mlp_gain: bfloat16 [2048], replicated, may hold values from 0.099609375 to 1.8984375
- w_up: bfloat16 [2048, 8192], P('kv', 'tp'), may hold values from -0.125 to 0.125
- w_down: bfloat16 [8192, 2048], P('tp', 'kv'), may hold values from -0.0625 to 0.0625
Outputs:
- result: bfloat16 [256, 2048], P('grp', ('kv', 'tp')), parts along dimension 0
- new_state: float32 [256, 32, 128, 128], P(('grp', 'kv'), 'tp'), parts along dimension 0
There are 2 independent parts, one for each index of `grp`. A program takes and returns all parts, laid end to end along the dimension named above; an argument that names none is the same for every part. Nothing has to cross between parts.
All inputs are finite; a program needn't handle non-finite values. No bound on the sum of `lengths` on one device may be relied on, other than what follows from the above.
Results may differ from a plain program's by a relative error of at most 0.01.
Values may be sent and summed in bfloat16 or wider, within the bound.
A program may use at most 64 MiB of HBM per device.

v0:
```python
import jax
import jax.numpy as jnp
from jax import lax
from jax.sharding import PartitionSpec as P

EPSILON = 1e-06


def from_everyone(array, axis):
    length = lax.axis_size(axis)
    return lax.all_to_all(
        jnp.broadcast_to(array[None], (length, *array.shape)), axis, 0, 0, tiled=True
    )


def laid_out(parts, dim):
    parts = jnp.moveaxis(parts, 0, dim)
    shape = parts.shape
    return parts.reshape(*shape[:dim], shape[dim] * shape[dim + 1], *shape[dim + 2 :])


def collect(array, axis, dim):
    parts = from_everyone(array, axis)
    return laid_out(parts, dim)


def cut_along(array, dim, length):
    before, after = (array.shape[:dim], array.shape[dim + 1 :])
    return jnp.moveaxis(array.reshape(*before, length, -1, *after), dim, 0)


def sent_and_summed(array, axis, dim):
    parts = cut_along(array, dim, lax.axis_size(axis))
    arrived = lax.all_to_all(parts, axis, split_axis=0, concat_axis=0, tiled=True)
    return arrived.sum(axis=0)


def side_by_side(arrays, axis, dim, along):
    both = jnp.concatenate(arrays, axis=along)
    out, at, done = (sent_and_summed(both, axis, dim), 0, [])
    for a in arrays:
        done.append(lax.slice_in_dim(out, at, at + a.shape[along], axis=along))
        at += a.shape[along]
    return tuple(done)


def taken_together(array, axis):
    return from_everyone(array, axis).sum(axis=0)


def unit_rows(values, factor):
    return values * lax.rsqrt(jnp.sum(values * values, axis=-1, keepdims=True) + EPSILON) * factor


def short_filter(current, history, weights, live_rows):
    history_live = jnp.where(live_rows[:, :, None], history.astype(jnp.float32), 0.0)
    filter_taps = weights.astype(jnp.float32)
    filtered = current * filter_taps[-1] + jnp.sum(history_live * filter_taps[None, :-1], axis=1)
    return jax.nn.silu(filtered)


def delta_step(delta_state, fresh_rows, queries, keys_now, values_now, strength, log_fade):
    fade_factor = jnp.exp(log_fade)[:, :, None, None]
    carried = jnp.where(fresh_rows[:, None, None, None], 0.0, delta_state) * fade_factor
    recalled = jnp.sum(carried * keys_now[:, :, :, None], axis=2)
    update = strength[:, :, None] * (values_now - recalled)
    new_state = carried + keys_now[:, :, :, None] * update[:, :, None, :]
    readout = jnp.sum(new_state * queries[:, :, :, None], axis=2)
    return (new_state, readout)


def gated_norm(readout, gain, gate_in):
    normed = readout * lax.rsqrt(jnp.mean(readout * readout, axis=-1, keepdims=True) + EPSILON)
    return (normed * gain.astype(jnp.float32) * jax.nn.silu(gate_in)).astype(jnp.bfloat16)


def block_squares(values):
    wide_values = values.astype(jnp.float32)
    return jnp.sum(wide_values * wide_values, axis=1, keepdims=True)


def scaled_rows(block_values, gain, block_first, block_cols):
    gain_block = lax.dynamic_slice_in_dim(gain, block_first, block_cols).astype(jnp.float32)
    return (block_values.astype(jnp.float32) * gain_block).astype(jnp.bfloat16)


def on_device(
    stream,
    lengths,
    delta_state,
    q_hist,
    k_hist,
    v_hist,
    norm_gain,
    w_query,
    w_key,
    w_value,
    w_gate,
    w_beta,
    w_decay,
    conv_query,
    conv_key,
    conv_value,
    decay_log,
    time_bias,
    out_gain,
    w_out,
    mlp_gain,
    w_up,
    w_down,
):
    model_width = norm_gain.shape[0]
    block_cols = model_width // lax.axis_size("kv")
    piece_cols = block_cols // lax.axis_size("tp")
    kv_place = lax.axis_index("kv")
    tp_place = lax.axis_index("tp")
    block_first = kv_place * block_cols
    own_count = delta_state.shape[0]
    heads_own = delta_state.shape[1]
    head_size = delta_state.shape[2]
    key_cols = q_hist.shape[2]
    value_cols = v_hist.shape[2]
    taps_count = q_hist.shape[1] + 1
    stream_block = collect(stream, "tp", 1)
    scaled = scaled_rows(stream_block, norm_gain, block_first, block_cols)

    def partial_value(weight):
        return jnp.dot(scaled, weight, preferred_element_type=jnp.float32)

    beta_rows = lax.dynamic_slice(
        w_beta, (block_first, tp_place * heads_own), (block_cols, heads_own)
    )
    decay_rows = lax.dynamic_slice(
        w_decay, (block_first, tp_place * heads_own), (block_cols, heads_own)
    )
    joined = jnp.concatenate(
        [
            partial_value(w_query),
            partial_value(w_key),
            partial_value(w_value),
            partial_value(w_gate),
        ],
        axis=1,
    )
    gate_terms = jnp.concatenate([partial_value(beta_rows), partial_value(decay_rows)], axis=1)
    joined, gate_terms, squares = side_by_side(
        (joined, gate_terms, block_squares(stream_block)), "kv", 0, 1
    )
    row_scale = lax.rsqrt(squares / model_width + EPSILON)
    joined = joined * row_scale
    gate_terms = gate_terms * row_scale
    live_rows = (
        jnp.arange(taps_count - 1, dtype=jnp.int32)[None, :] >= (taps_count - lengths)[:, None]
    )

    def own_taps(weights, columns):
        return lax.dynamic_slice_in_dim(weights, tp_place * columns, columns, 1)

    queries = short_filter(joined[:, :key_cols], q_hist, own_taps(conv_query, key_cols), live_rows)
    keys_now = short_filter(
        joined[:, key_cols : 2 * key_cols], k_hist, own_taps(conv_key, key_cols), live_rows
    )
    values_now = short_filter(
        joined[:, 2 * key_cols : 2 * key_cols + value_cols],
        v_hist,
        own_taps(conv_value, value_cols),
        live_rows,
    )
    gate_in = joined[:, 2 * key_cols + value_cols :].reshape(own_count, heads_own, head_size)
    key_heads = key_cols // head_size
    repeat_count = heads_own // key_heads
    queries = jnp.repeat(
        unit_rows(queries.reshape(own_count, key_heads, head_size), head_size ** (-0.5)),
        repeat_count,
        axis=1,
    )
    keys_now = jnp.repeat(
        unit_rows(keys_now.reshape(own_count, key_heads, head_size), 1.0), repeat_count, axis=1
    )
    values_now = values_now.reshape(own_count, heads_own, head_size)
    strength = jax.nn.sigmoid(gate_terms[:, :heads_own])
    decay_rates = lax.dynamic_slice_in_dim(decay_log, tp_place * heads_own, heads_own)
    biases = lax.dynamic_slice_in_dim(time_bias, tp_place * heads_own, heads_own)
    log_fade = -jnp.exp(decay_rates) * jax.nn.softplus(gate_terms[:, heads_own:] + biases)
    new_state, readout = delta_step(
        delta_state, lengths == 1, queries, keys_now, values_now, strength, log_fade
    )
    gated = gated_norm(readout, out_gain, gate_in).reshape(own_count, value_cols)
    mixer_part = jnp.dot(collect(gated, "kv", 0), w_out, preferred_element_type=jnp.float32)
    mixer_block = taken_together(mixer_part, "tp")
    mixed_block = (stream_block.astype(jnp.float32) + mixer_block).astype(jnp.bfloat16)
    mixed_own = lax.dynamic_slice_in_dim(mixed_block, tp_place * piece_cols, piece_cols, 1)
    scaled_mix = scaled_rows(mixed_block, mlp_gain, block_first, block_cols)
    unit_terms = jnp.dot(scaled_mix, w_up, preferred_element_type=jnp.float32)
    unit_terms, squares = side_by_side((unit_terms, block_squares(mixed_block)), "kv", 0, 1)
    unit_scale = lax.rsqrt(squares / model_width + EPSILON)
    hidden = jnp.square(jax.nn.relu(unit_terms * unit_scale)).astype(jnp.bfloat16)
    down_part = jnp.dot(collect(hidden, "kv", 0), w_down, preferred_element_type=jnp.float32)
    down_own = sent_and_summed(down_part, "tp", 1)
    result = (mixed_own.astype(jnp.float32) + down_own).astype(jnp.bfloat16)
    return (result, new_state)


def solution(mesh):
    in_specs = (
        P("grp", ("kv", "tp")),
        P(("grp", "kv")),
        P(("grp", "kv"), "tp", None, None),
        P(("grp", "kv"), None, "tp"),
        P(("grp", "kv"), None, "tp"),
        P(("grp", "kv"), None, "tp"),
        P(),
        P("kv", "tp"),
        P("kv", "tp"),
        P("kv", "tp"),
        P("kv", "tp"),
        P(),
        P(),
        P(),
        P(),
        P(),
        P(),
        P(),
        P(),
        P("tp", "kv"),
        P(),
        P("kv", "tp"),
        P("tp", "kv"),
    )
    out_specs = (P("grp", ("kv", "tp")), P(("grp", "kv"), "tp", None, None))
    return jax.shard_map(
        on_device, mesh=mesh, in_specs=in_specs, out_specs=out_specs, check_vma=False
    )
```

profile of v0, /device:TPU:33, one launch (start us, length us, event | category | flops | bytes accessed | tf_op | source)
XLA Modules:
  0.0 198.7 jit_solution(9255008714055168548)
XLA Ops:
  0.7 1.4 broadcast_in_dim.52
  2.0 23.7 %all-to-all-start = ((bf16[8,128,16]{1,2,0:T(8,128)(2,1)}), bf16[8,128,16]{1,2,0:T(8,128)(2,1)S(1)}, u32[]{:S(2)}, u32[]{:S(2)}) async-start(bf16[8,128,16]{1,2,0:T(8,128)(2,1)} %broadcast_in_dim.52), calls=%async_computation | async-start | bytes 65536 | tf_op jit(solution)/shard_map/all_to_all | solution.py:11
  26.5 4.0 %all-to-all-done = bf16[8,128,16]{1,2,0:T(8,128)(2,1)S(1)} async-done(((bf16[8,128,16]{1,2,0:T(8,128)(2,1)}), bf16[8,128,16]{1,2,0:T(8,128)(2,1)S(1)}, u32[]{:S(2)}, u32[]{:S(2)}) %all-to-all-start) | async-done | bytes 32800 | tf_op jit(solution)/shard_map/all_to_all | solution.py:11
  31.0 0.9 fusion.37
  31.8 0.9 fusion.39
  32.7 1.1 fusion.5
  34.6 1.0 concatenate.13
  35.6 6.0 %all-to-all-start.1 = ((f32[16,8,1545]{2,1,0:T(8,128)}), f32[16,8,1545]{2,1,0:T(8,128)S(1)}, u32[]{:S(2)}, u32[]{:S(2)}) async-start(f32[16,8,1545]{2,1,0:T(8,128)} %concatenate.13), calls=%async_computation.1 | async-start | bytes 1703936 | tf_op jit(solution)/shard_map/all_to_all | solution.py:34
  41.6 1.3 dynamic_slice.34
  45.6 1.2 exponential_negate_fusion
  48.3 29.9 %all-to-all-done.1 = f32[16,8,1545]{2,1,0:T(8,128)S(1)} async-done(((f32[16,8,1545]{2,1,0:T(8,128)}), f32[16,8,1545]{2,1,0:T(8,128)S(1)}, u32[]{:S(2)}, u32[]{:S(2)}) %all-to-all-start.1) | async-done | bytes 791072 | tf_op jit(solution)/shard_map/all_to_all | solution.py:34
  79.5 0.8 add_divide_fusion
  80.3 0.8 multiply_reduce_fusion.1
  81.3 2.3 %multiply_reduce_fusion = (f32[8,4,128]{2,1,0:T(4,128)S(1)}, f32[8,4,128,128]{3,2,1,0:T(8,128)}) fusion(f32[8,4,128]{2,1,0:T(4,128)S(1)} %bitcast.95, f32[8,4,128]{2,1,0:T(4,128)S(1)} %fusion.23, f32[8,4,128]{2,1,0:T(4,128)S(1)} %bitcast.93, f32[8,4]{1,0:T(8,128)S(1)} %get-tuple-element.19, f32[8,4,128,128]{3,2,1,0:T(8,128)S(1)} %copy-done.1, ...), kind=kLoop, calls=%fused_computation | loop fusion | flops 3141632 | bytes 4259976 | tf_op jit(solution)/shard_map/reduce_sum | solution.py:68
  83.8 24.6 %all_to_all.35 = bf16[16,8,512]{2,1,0:T(8,128)(2,1)S(1)} all-to-all(bf16[16,8,512]{2,1,0:T(8,128)(2,1)S(1)} %broadcast_in_dim.61), channel_id=1, replica_groups=mesh['grp'=2,'kv'=16,'tp'=8] {'kv'}, dimensions={0} | all-to-all | bytes 262144 | tf_op jit(solution)/shard_map/all_to_all | solution.py:11
  108.6 0.8 broadcast_in_dim.62
  109.4 6.8 %all-to-all-start.3 = ((f32[8,128,128]{2,1,0:T(8,128)}), f32[8,128,128]{2,1,0:T(8,128)S(1)}, u32[]{:S(2)}, u32[]{:S(2)}) async-start(f32[8,128,128]{2,1,0:T(8,128)} %broadcast_in_dim.62), calls=%async_computation.3 | async-start | bytes 1048576 | tf_op jit(solution)/shard_map/all_to_all | solution.py:11
  116.9 8.7 %all-to-all-done.3 = f32[8,128,128]{2,1,0:T(8,128)S(1)} async-done(((f32[8,128,128]{2,1,0:T(8,128)}), f32[8,128,128]{2,1,0:T(8,128)S(1)}, u32[]{:S(2)}, u32[]{:S(2)}) %all-to-all-start.3) | async-done | bytes 524320 | tf_op jit(solution)/shard_map/all_to_all | solution.py:11
  126.3 36.2 %all_to_all.36 = f32[16,8,1025]{2,1,0:T(8,128)S(1)} all-to-all(f32[16,8,1025]{2,1,0:T(8,128)S(1)} %pad_maximum_fusion), channel_id=1, replica_groups=mesh['grp'=2,'kv'=16,'tp'=8] {'kv'}, dimensions={0} | all-to-all | bytes 1049600 | tf_op jit(solution)/shard_map/all_to_all | solution.py:34
  163.5 5.9 %all-to-all-start.5 = ((bf16[16,8,1024]{2,1,0:T(8,128)(2,1)}), bf16[16,8,1024]{2,1,0:T(8,128)(2,1)S(1)}, u32[]{:S(2)}, u32[]{:S(2)}) async-start(bf16[16,8,1024]{2,1,0:T(8,128)(2,1)} %broadcast_in_dim.102), calls=%async_computation.5 | async-start | bytes 524288 | tf_op jit(solution)/shard_map/all_to_all | solution.py:11
  169.5 12.4 %all-to-all-done.5 = bf16[16,8,1024]{2,1,0:T(8,128)(2,1)S(1)} async-done(((bf16[16,8,1024]{2,1,0:T(8,128)(2,1)}), bf16[16,8,1024]{2,1,0:T(8,128)(2,1)S(1)}, u32[]{:S(2)}, u32[]{:S(2)}) %all-to-all-start.5) | async-done | bytes 262176 | tf_op jit(solution)/shard_map/all_to_all | solution.py:11
  181.9 0.9 convolution_bitcast_fusion
  182.7 10.2 %all-to-all-start.6 = ((f32[8,128,16]{1,2,0:T(8,128)}), f32[8,128,16]{1,2,0:T(8,128)S(1)}, u32[]{:S(2)}, u32[]{:S(2)}) async-start(f32[8,128,16]{1,2,0:T(8,128)} %convolution_bitcast_fusion), calls=%async_computation.6 | async-start | bytes 131072 | tf_op jit(solution)/shard_map/all_to_all | solution.py:34
  193.0 4.8 %all-to-all-done.6 = f32[8,128,16]{1,2,0:T(8,128)S(1)} async-done(((f32[8,128,16]{1,2,0:T(8,128)}), f32[8,128,16]{1,2,0:T(8,128)S(1)}, u32[]{:S(2)}, u32[]{:S(2)}) %all-to-all-start.6) | async-done | bytes 65568 | tf_op jit(solution)/shard_map/all_to_all | solution.py:34
  (80 shorter events, 11.3 us)
Async XLA Ops:
  0.6 125.4 %copy-start = (bf16[128,1024]{1,0:T(8,128)(2,1)S(1)}, bf16[128,1024]{1,0:T(8,128)(2,1)}, u32[]{:S(2)}) copy-start(bf16[128,1024]{1,0:T(8,128)(2,1)} %param.44) | copy-start | bytes 786436
  0.6 33.1 %copy-start.3 = (bf16[128,512]{1,0:T(8,128)(2,1)S(1)}, bf16[128,512]{1,0:T(8,128)(2,1)}, u32[]{:S(2)}) copy-start(bf16[128,512]{1,0:T(8,128)(2,1)} %param.32) | copy-start | bytes 393220
  0.7 33.3 %copy-start.5 = (bf16[128,256]{1,0:T(8,128)(2,1)S(1)}, bf16[128,256]{1,0:T(8,128)(2,1)}, u32[]{:S(2)}) copy-start(bf16[128,256]{1,0:T(8,128)(2,1)} %param.31) | copy-start | bytes 196612
  0.7 33.5 %copy-start.6 = (bf16[128,256]{1,0:T(8,128)(2,1)S(1)}, bf16[128,256]{1,0:T(8,128)(2,1)}, u32[]{:S(2)}) copy-start(bf16[128,256]{1,0:T(8,128)(2,1)} %param.30) | copy-start | bytes 196612
  2.0 28.4 %all-to-all-start = ((bf16[8,128,16]{1,2,0:T(8,128)(2,1)}), bf16[8,128,16]{1,2,0:T(8,128)(2,1)S(1)}, u32[]{:S(2)}, u32[]{:S(2)}) async-start(bf16[8,128,16]{1,2,0:T(8,128)(2,1)} %broadcast_in_dim.52), calls=%async_computation | async-start | bytes 65536 | tf_op jit(solution)/shard_map/all_to_all | solution.py:11
  34.0 13.5 %copy-start.7 = (bf16[8,3,512]{2,0,1:T(8,128)(2,1)S(1)}, bf16[8,3,512]{2,0,1:T(8,128)(2,1)}, u32[]{:S(2)}) copy-start(bf16[8,3,512]{2,0,1:T(8,128)(2,1)} %param.28) | copy-start | bytes 73732
  34.0 13.5 %copy-start.8 = (bf16[8,3,256]{2,0,1:T(8,128)(2,1)S(1)}, bf16[8,3,256]{2,0,1:T(8,128)(2,1)}, u32[]{:S(2)}) copy-start(bf16[8,3,256]{2,0,1:T(8,128)(2,1)} %param.26) | copy-start | bytes 36868
  34.0 13.5 %copy-start.9 = (bf16[8,3,256]{2,0,1:T(8,128)(2,1)S(1)}, bf16[8,3,256]{2,0,1:T(8,128)(2,1)}, u32[]{:S(2)}) copy-start(bf16[8,3,256]{2,0,1:T(8,128)(2,1)} %param.27) | copy-start | bytes 36868
  34.6 45.7 %copy-start.1 = (f32[8,4,128,128]{3,2,1,0:T(8,128)S(1)}, f32[8,4,128,128]{3,2,1,0:T(8,128)}, u32[]{:S(2)}) copy-start(f32[8,4,128,128]{3,2,1,0:T(8,128)} %param.25) | copy-start | bytes 6291460
  35.6 42.6 %all-to-all-start.1 = ((f32[16,8,1545]{2,1,0:T(8,128)}), f32[16,8,1545]{2,1,0:T(8,128)S(1)}, u32[]{:S(2)}, u32[]{:S(2)}) async-start(f32[16,8,1545]{2,1,0:T(8,128)} %concatenate.13), calls=%async_computation.1 | async-start | bytes 1703936 | tf_op jit(solution)/shard_map/all_to_all | solution.py:34
  81.3 27.2 %copy-start.4 = (bf16[512,128]{1,0:T(8,128)(2,1)S(1)}, bf16[512,128]{1,0:T(8,128)(2,1)}, u32[]{:S(2)}) copy-start(bf16[512,128]{1,0:T(8,128)(2,1)} %param.42) | copy-start | bytes 393220
  109.4 16.2 %all-to-all-start.3 = ((f32[8,128,128]{2,1,0:T(8,128)}), f32[8,128,128]{2,1,0:T(8,128)S(1)}, u32[]{:S(2)}, u32[]{:S(2)}) async-start(f32[8,128,128]{2,1,0:T(8,128)} %broadcast_in_dim.62), calls=%async_computation.3 | async-start | bytes 1048576 | tf_op jit(solution)/shard_map/all_to_all | solution.py:11
  126.2 43.1 %copy-start.2 = (bf16[1024,128]{1,0:T(8,128)(2,1)S(1)}, bf16[1024,128]{1,0:T(8,128)(2,1)}, u32[]{:S(2)}) copy-start(bf16[1024,128]{1,0:T(8,128)(2,1)} %param.45) | copy-start | bytes 786436
  163.5 18.4 %all-to-all-start.5 = ((bf16[16,8,1024]{2,1,0:T(8,128)(2,1)}), bf16[16,8,1024]{2,1,0:T(8,128)(2,1)S(1)}, u32[]{:S(2)}, u32[]{:S(2)}) async-start(bf16[16,8,1024]{2,1,0:T(8,128)(2,1)} %broadcast_in_dim.102), calls=%async_computation.5 | async-start | bytes 524288 | tf_op jit(solution)/shard_map/all_to_all | solution.py:11
  182.7 15.1 %all-to-all-start.6 = ((f32[8,128,16]{1,2,0:T(8,128)}), f32[8,128,16]{1,2,0:T(8,128)S(1)}, u32[]{:S(2)}, u32[]{:S(2)}) async-start(f32[8,128,16]{1,2,0:T(8,128)} %convolution_bitcast_fusion), calls=%async_computation.6 | async-start | bytes 131072 | tf_op jit(solution)/shard_map/all_to_all | solution.py:34
where the time goes:
time: 200 us; the launch traced here: 199 us
  blocking collectives  60.8 us (30%)
  waiting for transfers between devices  59.8 us (30%)
  starting transfers between devices  52.4 us (26%)
  other arithmetic  12.3 us (6%)
  local copies, waits for them, and re-layouts  7.88 us (4%)
  matrix products  4.54 us (2%)
    all_to_all x3, starting transfers between devices, from_everyone(): lax.all_to_all(jnp.broadcast_to(array[None], (length, *array.shape)), axi...  36.3 us
    all_to_all x1, blocking collectives, sent_and_summed(): lax.all_to_all(parts, axis, split_axis=0, concat_axis=0, tiled=True)  36.2 us
    all_to_all x2, waiting for transfers between devices, sent_and_summed(): lax.all_to_all(parts, axis, split_axis=0, concat_axis=0, tiled=True)  34.7 us
    all_to_all x3, waiting for transfers between devices, from_everyone(): lax.all_to_all(jnp.broadcast_to(array[None], (length, *array.shape)), axi...  25.1 us
    all_to_all x1, blocking collectives, from_everyone(): lax.all_to_all(jnp.broadcast_to(array[None], (length, *array.shape)), axi...  24.6 us
    all_to_all x2, starting transfers between devices, sent_and_summed(): lax.all_to_all(parts, axis, split_axis=0, concat_axis=0, tiled=True)  16.1 us
  transfers between devices with their start and end apart: 5, of which 5 were waited for; matrix products, arithmetic and copies ran while one was open for 4% of the time, Pallas kernels for 0%

commit v1 on v0

v1 whole, which is shorter than its diff:
```python
import functools
import types
import typing

import jax
import jax.numpy as jnp
from jax import lax
from jax.experimental import pallas as pl
from jax.experimental.pallas import tpu as pltpu
from jax.sharding import PartitionSpec as P

EPSILON = 1e-06
LANES = 128
MESH = pl.DeviceIdType.MESH
F32 = jnp.float32
BF16 = jnp.bfloat16

class Inputs(typing.NamedTuple):
    stream: typing.Any
    lengths: typing.Any
    delta_state: typing.Any
    q_hist: typing.Any
    k_hist: typing.Any
    v_hist: typing.Any
    norm_gain: typing.Any
    w_query: typing.Any
    w_key: typing.Any
    w_value: typing.Any
    w_gate: typing.Any
    w_beta: typing.Any
    w_decay: typing.Any
    conv_query: typing.Any
    conv_key: typing.Any
    conv_value: typing.Any
    decay_log: typing.Any
    time_bias: typing.Any
    out_gain: typing.Any
    w_out: typing.Any
    mlp_gain: typing.Any
    w_up: typing.Any
    w_down: typing.Any


def ring_offsets(n):
    return list(range(1, n // 2 + 1)) + [-o for o in range(1, (n + 1) // 2)]


def tree(n, relayed):
    return {o: (o - (1 if o > 0 else -1)) if abs(o) in relayed else 0 for o in ring_offsets(n)}


def children_of(parents, o):
    return [c for c, p in parents.items() if p == o]


def depth_of(parents, o):
    return 0 if o == 0 else 1 + depth_of(parents, parents[o])


class Exchange:
    def __init__(self, axis, n, place, send_sems, recv_sems):
        self.axis, self.n, self.place = axis, n, place
        self.send_sems, self.recv_sems = send_sems, recv_sems
        self.started = []

    def at(self, o):
        return lax.rem(self.place + (o + self.n), self.n)

    def copy(self, key, hop, src, dst):
        slot = key % self.n
        return pltpu.make_async_remote_copy(
            src_ref=src,
            dst_ref=dst,
            send_sem=self.send_sems.at[slot],
            recv_sem=self.recv_sems.at[slot],
            device_id={self.axis: self.at(hop)},
            device_id_type=MESH,
        )

    def start(self, key, hop, src, dst):
        copy = self.copy(key, hop, src, dst)
        copy.start()
        self.started.append(copy)

    def wait(self, key, src, dst):
        self.copy(key, 1, src, dst).wait_recv()

    def drain(self):
        for copy in self.started:
            copy.wait_send()
        self.started = []


class Scatter:
    def __init__(self, exchange, parents, part, send, recv):
        self.x, self.parents = exchange, parents
        self.part, self.send, self.recv = part, send, recv
        self.inner = [o for o in parents if children_of(parents, o)]
        self.inner.sort(key=lambda o: (-depth_of(parents, o), -abs(o)))

    def _send(self, o, value):
        slot = o % self.x.n
        self.send[slot] = value.astype(BF16)
        self.x.start(o, o - self.parents[o], self.send.at[slot], self.recv.at[slot])

    def _gather(self, o):
        total = self.part[o % self.x.n]
        for c in children_of(self.parents, o):
            slot = c % self.x.n
            self.x.wait(c, self.send.at[slot], self.recv.at[slot])
            total = total + self.recv[slot].astype(F32)
        return total

    def leaves(self, relayed):
        for o in sorted(self.parents, key=lambda o: -abs(o)):
            if o not in self.inner and (self.parents[o] != 0) == relayed:
                self._send(o, self.part[o % self.x.n])

    def hubs(self):
        for o in self.inner:
            self._send(o, self._gather(o))

    def total(self):
        return self._gather(0)


class Gather:
    def __init__(self, exchange, parents, blocks):
        self.x, self.parents, self.blocks = exchange, parents, blocks

    def _forward(self, o):
        source = self.blocks.at[self.x.at(-o)]
        for c in sorted(children_of(self.parents, o), key=lambda c: -abs(c)):
            self.x.start(c, c - o, source, source)

    def begin(self):
        self._forward(0)

    def finish(self):
        order = sorted(self.parents, key=lambda o: (not children_of(self.parents, o), abs(o)))
        for o in order:
            block = self.blocks.at[self.x.at(-o)]
            self.x.wait(o, block, block)
            self._forward(o)


def rows_of(blocks):
    return blocks.reshape(blocks.shape[0] * blocks.shape[1], blocks.shape[2])


def softplus(x):
    return jnp.maximum(x, 0.0) + jnp.log1p(jnp.exp(-jnp.abs(x)))


class Phases:
    def __init__(self):
        self.scope = None

    def __call__(self, label):
        self.end()
        self.scope = jax.named_scope(label)
        self.scope.__enter__()

    def end(self):
        if self.scope is not None:
            self.scope.__exit__(None, None, None)
        self.scope = None


def layer(d, a, result, new_state, v, r):
    n_kv, n_tp = d.n_kv, d.n_tp
    own, heads, size = d.own, d.heads, d.size
    key_cols, value_cols, ff = d.key_cols, d.value_cols, d.ff
    width, block, piece, taps = d.width, d.block, d.piece, d.taps
    heads_all, seqs = d.heads_all, d.own * d.n_kv
    kv, tp = lax.axis_index("kv"), lax.axis_index("tp")
    phase = Phases()
    phase("enter")

    def over_kv(sems):
        return Exchange("kv", n_kv, kv, *sems)

    def over_tp(sems):
        return Exchange("tp", n_tp, tp, *sems)

    x_stream = over_tp(r.stream_sems)
    x_proj = over_kv(r.proj_sems)
    barrier = pltpu.get_barrier_semaphore()
    for o in range(1, n_tp):
        pl.semaphore_signal(barrier, 1, device_id={"tp": x_stream.at(o)}, device_id_type=MESH)
    for o in (1, -1):
        pl.semaphore_signal(barrier, 1, device_id={"kv": x_proj.at(o)}, device_id_type=MESH)

    started = []

    def load(source, into):
        copy = pltpu.make_async_copy(source, into, r.load_sems.at[len(started)])
        copy.start()
        started.append(copy)
        return copy

    def tp_cols(ref, count):
        return ref.at[:, pl.ds(pl.multiple_of(tp * count, LANES), count)]

    def kv_cols(ref):
        return ref.at[:, pl.ds(pl.multiple_of(kv * block, LANES), block)]

    sources = a._replace(
        w_beta=kv_cols(a.w_beta),
        w_decay=kv_cols(a.w_decay),
        conv_query=tp_cols(a.conv_query, key_cols),
        conv_key=tp_cols(a.conv_key, key_cols),
        conv_value=tp_cols(a.conv_value, value_cols),
    )
    first = Inputs(*range(len(a)))
    order = [first.stream, first.norm_gain, first.w_decay, first.w_beta]
    order += [first.w_query, first.w_key, first.w_value, first.w_gate]
    order += [i for i in range(len(a)) if i not in order]
    order.remove(first.delta_state)
    order.append(first.delta_state)
    copies = {i: load(sources[i], v[i]) for i in order}
    c = Inputs(*[copies[i] for i in range(len(a))])

    c.stream.wait()
    pieces = r.pieces
    pieces[tp] = v.stream[...]
    pl.semaphore_wait(barrier, n_tp - 1 + 2)

    def tell(step):
        sem = r.near_sems.at[step.bit_length() - 1]
        for o in (step, -step):
            pl.semaphore_signal(sem, 1, device_id={"kv": x_proj.at(o)}, device_id_type=MESH)

    def heard(step):
        pl.semaphore_wait(r.near_sems.at[step.bit_length() - 1], 2)

    g_stream = Gather(x_stream, {o: 0 for o in ring_offsets(n_tp)}, pieces)
    g_stream.begin()
    tell(1)

    def gain_row(copy, ref):
        copy.wait()
        gains = ref[...].astype(F32)
        row = lax.broadcasted_iota(jnp.int32, gains.shape, 0)
        return jnp.sum(jnp.where(row == kv, gains, 0.0), axis=0, keepdims=True)

    norm_row = gain_row(c.norm_gain, v.norm_gain)
    c.w_decay.wait()
    c.w_beta.wait()
    idle = jnp.zeros((LANES - 2 * heads_all, block), F32)
    w_rates = [v.w_decay[...].astype(F32), v.w_beta[...].astype(F32), idle]
    w_rates = jnp.concatenate(w_rates, axis=0).astype(BF16)
    for copy in (c.w_query, c.w_key, c.w_value, c.w_gate):
        copy.wait()

    parents = d.scatter_tree
    order = [0] + list(parents)

    def by_owner(values):
        r.rows[...] = values.reshape(n_kv, own, block)
        return jnp.concatenate([r.rows[x_proj.at(o)] for o in order], axis=0)

    def put(part, at, product):
        parts = product.reshape(n_kv, own, product.shape[1])
        for i, o in enumerate(order):
            part[o % n_kv, :, at : at + product.shape[1]] = parts[i]

    def spread_squares(values):
        squares = jnp.sum(values * values, axis=1, keepdims=True)
        return by_owner(jnp.broadcast_to(squares, values.shape))

    phase("stream")
    g_stream.finish()
    phase("project")
    stream_block = rows_of(pieces[...].astype(F32)).T
    r.stream_block[...] = stream_block
    lhs = by_owner((stream_block * norm_row).astype(BF16).astype(F32)).astype(BF16)
    at = 0
    for weight in (v.w_query, v.w_key, v.w_value):
        product = jnp.dot(lhs, weight[...], preferred_element_type=F32)
        put(r.part_a, at, product)
        at += product.shape[1]
    rates = lax.dot_general(lhs, w_rates, (((1,), (1,)), ((), ())), preferred_element_type=F32)
    lane = lax.broadcasted_iota(jnp.int32, rates.shape, 1)
    put(r.part_a, at, jnp.where(lane < 2 * heads_all, rates, spread_squares(stream_block)))
    s_proj = Scatter(x_proj, parents, r.part_a, r.send_a, r.recv_a)
    s_proj.leaves(True)
    heard(1)
    tell(2)
    put(r.part_g, 0, jnp.dot(lhs, v.w_gate[...], preferred_element_type=F32))
    s_gate = Scatter(over_kv(r.gate_sems), parents, r.part_g, r.send_g, r.recv_g)
    heard(2)
    tell(4)

    phase("history")
    c.lengths.wait()
    seq = lax.broadcasted_iota(jnp.int32, (own, LANES), 0)
    lens = jnp.zeros((own, LANES), jnp.int32)
    for s in range(own):
        lens = jnp.where(seq == s, v.lengths[s], lens)

    def history(past_copy, past, weight_copy, weight):
        past_copy.wait()
        weight_copy.wait()
        weights = weight[...].astype(F32)
        count = weights.shape[1]
        wide = jnp.concatenate([lens] * (count // LANES), axis=1)
        total = jnp.zeros((own, count), F32)
        for i in range(taps - 1):
            term = past[i].astype(F32) * weights[i : i + 1, :]
            total = total + jnp.where(wide >= taps - i, term, 0.0)
        return total, weights[taps - 1 : taps, :]

    q_past, q_tap = history(c.q_hist, v.q_hist, c.conv_query, v.conv_query)
    k_past, k_tap = history(c.k_hist, v.k_hist, c.conv_key, v.conv_key)
    v_past, v_tap = history(c.v_hist, v.v_hist, c.conv_value, v.conv_value)
    c.out_gain.wait()
    gain_out = v.out_gain[...].astype(F32)
    c.decay_log.wait()
    c.time_bias.wait()
    rate = jnp.exp(v.decay_log[...])
    bias = v.time_bias[...]
    mlp_row = gain_row(c.mlp_gain, v.mlp_gain)

    heard(4)
    phase("hubs")
    s_proj.leaves(False)
    s_proj.hubs()
    s_gate.leaves(True)
    s_gate.leaves(False)
    phase("gate_hubs")
    s_gate.hubs()
    for copy in (c.w_out, c.w_up, c.w_down, c.delta_state):
        copy.wait()

    phase("sums")
    sums = s_proj.total()
    phase("delta")
    at_v = 2 * key_cols
    misc = sums[:, at_v + value_cols :]
    scale = lax.rsqrt(misc[:, LANES - 1 : LANES] / width + EPSILON)
    misc = misc * scale

    def filtered(at, past, tap):
        value = sums[:, at : at + past.shape[1]] * scale * tap + past
        return value * jax.nn.sigmoid(value)

    def unit(values):
        return values * lax.rsqrt(jnp.sum(values * values, axis=-1, keepdims=True) + EPSILON)

    filtered_q = filtered(0, q_past, q_tap)
    filtered_k = filtered(key_cols, k_past, k_tap)
    values_now = filtered(at_v, v_past, v_tap)
    fade_all = jnp.exp(-rate * softplus(misc[:, :heads_all] + bias))
    strength_all = jax.nn.sigmoid(misc)

    def own_head(table, at):
        lanes = lax.broadcasted_iota(jnp.int32, table.shape, 1)
        one = jnp.sum(jnp.where(lanes == at, table, 0.0), axis=1, keepdims=True)
        return jnp.broadcast_to(one, (own, size))

    key_heads = key_cols // size
    repeat = heads // key_heads
    state = v.delta_state
    fades, strengths = [], []
    for h in range(heads):
        fades.append(jnp.where(lens == 1, 0.0, own_head(fade_all, tp * heads + h)))
        strengths.append(own_head(strength_all, heads_all + tp * heads + h))
    queries, keys, meets = [], [], []
    for g in range(key_heads):
        queries.append(unit(filtered_q[:, g * size : (g + 1) * size]) * size ** (-0.5))
        keys.append(unit(filtered_k[:, g * size : (g + 1) * size]))
        meet = jnp.sum(queries[g] * keys[g], axis=1, keepdims=True)
        meets.append(jnp.broadcast_to(meet, (own, size)))
    out_copies = []
    for s in range(own):
        for g in range(key_heads):
            key_wide = jnp.broadcast_to(keys[g][s : s + 1], (size, size)).T
            query_wide = jnp.broadcast_to(queries[g][s : s + 1], (size, size)).T
            for h in range(g * repeat, (g + 1) * repeat):
                held = state[s, h]
                fade = fades[h][s : s + 1]
                value = values_now[s : s + 1, h * size : (h + 1) * size]
                recalled = fade * jnp.sum(held * key_wide, axis=0, keepdims=True)
                update = strengths[h][s : s + 1] * (value - recalled)
                read = fade * jnp.sum(held * query_wide, axis=0, keepdims=True)
                r.readout[h, s : s + 1, :] = read + meets[g][s : s + 1] * update
                state[s, h] = fade * held + key_wide * update
        copy = pltpu.make_async_copy(state.at[s], new_state.at[s], r.out_sems.at[s])
        copy.start()
        out_copies.append(copy)

    phase("gated")
    gate_in = s_gate.total() * scale
    gated = []
    for h in range(heads):
        read = r.readout[h]
        mean = jnp.mean(read * read, axis=1, keepdims=True)
        gate = gate_in[:, h * size : (h + 1) * size]
        gate = gate * jax.nn.sigmoid(gate)
        gated.append(read * lax.rsqrt(mean + EPSILON) * gain_out * gate)
    r.all_gated[kv] = jnp.concatenate(gated, axis=1).astype(BF16)
    g_gated = Gather(over_kv(r.gated_sems), d.gated_tree, r.all_gated)
    g_gated.begin()
    phase("gather_gated")
    g_gated.finish()

    phase("mixer")

    def whole(blocks):
        return rows_of(blocks[...].astype(F32)).astype(BF16)

    mixer = jnp.dot(whole(r.all_gated), v.w_out[...], preferred_element_type=F32)
    r.mixers[0] = mixer.astype(BF16)
    x_mixer = over_tp(r.mixer_sems)
    others = sorted(ring_offsets(n_tp), key=lambda o: -abs(o))
    for o in others:
        x_mixer.start(o, o, r.mixers.at[0], r.mixers.at[o % n_tp])
    phase("sum_mixer")
    for o in reversed(others):
        x_mixer.wait(o, r.mixers.at[0], r.mixers.at[o % n_tp])
        mixer = mixer + r.mixers[o % n_tp].astype(F32)
    phase("up")
    mixed = (r.stream_block[...] + mixer).astype(BF16).astype(F32)
    r.mixed_turned[...] = mixed.T.reshape(n_tp, piece, seqs)

    lhs = by_owner((mixed * mlp_row).astype(BF16).astype(F32)).astype(BF16)
    put(r.part_u, 0, jnp.dot(lhs, v.w_up[...], preferred_element_type=F32))
    put(r.part_u, ff, spread_squares(mixed))
    s_up = Scatter(over_kv(r.up_sems), parents, r.part_u, r.send_u, r.recv_u)
    s_up.leaves(True)
    s_up.leaves(False)
    phase("up_hubs")
    s_up.hubs()
    phase("up_sums")
    sums = s_up.total()
    phase("hidden")
    unit_scale = lax.rsqrt(sums[:, ff : ff + 1] / width + EPSILON)
    raised = jnp.maximum(sums[:, :ff] * unit_scale, 0.0)
    r.all_hidden[kv] = (raised * raised).astype(BF16)
    g_hidden = Gather(over_kv(r.hidden_sems), d.hidden_tree, r.all_hidden)
    g_hidden.begin()
    phase("gather_hidden")
    g_hidden.finish()
    phase("down")
    down = lax.dot_general(
        v.w_down[...], whole(r.all_hidden), (((0,), (1,)), ((), ())), preferred_element_type=F32
    )
    down = down.reshape(n_tp, piece, seqs)
    r.down_wide[...] = down
    r.downs[...] = down.astype(BF16)
    x_down = over_tp(r.down_sems)
    for o in others:
        x_down.start(o, o, r.downs.at[x_down.at(o)], r.arrived.at[o % n_tp])
    phase("sum_down")
    total = r.down_wide[tp]
    for o in reversed(others):
        x_down.wait(o, r.downs.at[0], r.arrived.at[o % n_tp])
        total = total + r.arrived[o % n_tp].astype(F32)
    phase("leave")
    r.result[...] = (r.mixed_turned[tp] + total).astype(BF16)
    copy = pltpu.make_async_copy(r.result, result, r.out_sems.at[own])
    copy.start()
    out_copies.append(copy)
    exchanges = (x_stream, x_proj, s_gate.x, g_gated.x, x_mixer, s_up.x, g_hidden.x, x_down)
    for exchange in exchanges:
        exchange.drain()
    for copy in out_copies:
        copy.wait()
    phase.end()


def on_device(n_kv, n_tp, *args):
    given = Inputs(*args)
    own, heads, size = given.delta_state.shape[:3]
    key_cols, value_cols = given.q_hist.shape[2], given.v_hist.shape[2]
    taps = given.q_hist.shape[1] + 1
    width = given.norm_gain.shape[0]
    block = width // n_kv
    piece = block // n_tp
    ff = given.w_up.shape[1]
    heads_all = given.w_beta.shape[1]
    seqs = own * n_kv
    given = given._replace(
        stream=given.stream.T,
        q_hist=given.q_hist.transpose(1, 0, 2),
        k_hist=given.k_hist.transpose(1, 0, 2),
        v_hist=given.v_hist.transpose(1, 0, 2),
        norm_gain=given.norm_gain.reshape(n_kv, block),
        mlp_gain=given.mlp_gain.reshape(n_kv, block),
        w_beta=given.w_beta.T,
        w_decay=given.w_decay.T,
        decay_log=given.decay_log.reshape(1, -1),
        time_bias=given.time_bias.reshape(1, -1),
        out_gain=given.out_gain.reshape(1, -1),
    )
    d = types.SimpleNamespace(
        n_kv=n_kv,
        n_tp=n_tp,
        own=own,
        heads=heads,
        size=size,
        key_cols=key_cols,
        value_cols=value_cols,
        ff=ff,
        width=width,
        block=block,
        piece=piece,
        taps=taps,
        heads_all=heads_all,
        scatter_tree=tree(n_kv, (2, 4, 6, 8)),
        gated_tree=tree(n_kv, ()),
        hidden_tree=tree(n_kv, (2, 4, 6)),
    )
    held = Inputs(*[pltpu.VMEM(x.shape, x.dtype) for x in given])
    held = held._replace(
        lengths=pltpu.SMEM(given.lengths.shape, given.lengths.dtype),
        w_beta=pltpu.VMEM((heads_all, block), BF16),
        w_decay=pltpu.VMEM((heads_all, block), BF16),
        conv_query=pltpu.VMEM((taps, key_cols), BF16),
        conv_key=pltpu.VMEM((taps, key_cols), BF16),
        conv_value=pltpu.VMEM((taps, value_cols), BF16),
    )
    wide_a = 2 * key_cols + value_cols + LANES
    wide_u = ff + LANES

    def sems(n):
        return (pltpu.SemaphoreType.DMA((n,)), pltpu.SemaphoreType.DMA((n,)))

    def wide(*shape):
        return pltpu.VMEM(shape, F32)

    def narrow(*shape):
        return pltpu.VMEM(shape, BF16)

    scratch = dict(
        stream_sems=sems(n_tp),
        proj_sems=sems(n_kv),
        gate_sems=sems(n_kv),
        gated_sems=sems(n_kv),
        mixer_sems=sems(n_tp),
        up_sems=sems(n_kv),
        hidden_sems=sems(n_kv),
        down_sems=sems(n_tp),
        load_sems=pltpu.SemaphoreType.DMA((len(given),)),
        out_sems=pltpu.SemaphoreType.DMA((own + 1,)),
        near_sems=pltpu.SemaphoreType.REGULAR((3,)),
        pieces=narrow(n_tp, piece, seqs),
        rows=wide(n_kv, own, block),
        stream_block=wide(seqs, block),
        part_a=wide(n_kv, own, wide_a),
        send_a=narrow(n_kv, own, wide_a),
        recv_a=narrow(n_kv, own, wide_a),
        part_g=wide(n_kv, own, value_cols),
        send_g=narrow(n_kv, own, value_cols),
        recv_g=narrow(n_kv, own, value_cols),
        readout=wide(heads, own, size),
        all_gated=narrow(n_kv, own, value_cols),
        mixers=narrow(n_tp, seqs, block),
        mixed_turned=wide(n_tp, piece, seqs),
        part_u=wide(n_kv, own, wide_u),
        send_u=narrow(n_kv, own, wide_u),
        recv_u=narrow(n_kv, own, wide_u),
        all_hidden=narrow(n_kv, own, ff),
        downs=narrow(n_tp, piece, seqs),
        down_wide=wide(n_tp, piece, seqs),
        arrived=narrow(n_tp, piece, seqs),
        result=narrow(piece, seqs),
    )

    def kernel(*refs):
        count = len(given)
        a, outs, v = Inputs(*refs[:count]), refs[count : count + 2], refs[count + 2]
        layer(d, a, *outs, v, types.SimpleNamespace(**refs[count + 3]))

    state = given.delta_state
    turned, new_state = pl.pallas_call(
        kernel,
        out_shape=(
            jax.ShapeDtypeStruct((piece, seqs), BF16),
            jax.ShapeDtypeStruct(state.shape, state.dtype),
        ),
        in_specs=[pl.BlockSpec(memory_space=pl.ANY)] * len(given),
        out_specs=[pl.BlockSpec(memory_space=pl.ANY)] * 2,
        scratch_shapes=(held, scratch),
        compiler_params=pltpu.CompilerParams(
            collective_id=0, has_side_effects=True, vmem_limit_bytes=67043328
        ),
        name="layer",
    )(*given)
    return (turned.T, new_state)


def solution(mesh):
    kv_tp, heads_of = P("kv", "tp"), P("tp", "kv")
    history = P(("grp", "kv"), None, "tp")
    state = P(("grp", "kv"), "tp", None, None)
    stream = P("grp", ("kv", "tp"))
    placed = Inputs(*[P()] * len(Inputs._fields))._replace(
        stream=stream,
        lengths=P(("grp", "kv")),
        delta_state=state,
        q_hist=history,
        k_hist=history,
        v_hist=history,
        w_query=kv_tp,
        w_key=kv_tp,
        w_value=kv_tp,
        w_gate=kv_tp,
        w_out=heads_of,
        w_up=kv_tp,
        w_down=heads_of,
    )
    return jax.shard_map(
        functools.partial(on_device, mesh.shape["kv"], mesh.shape["tp"]),
        mesh=mesh,
        in_specs=tuple(placed),
        out_specs=(stream, state),
        check_vma=False,
    )
```

time: 200 us -> 96.5 us (0.48)
  Pallas kernels: 0 us -> 91.3 us
  blocking collectives: 60.8 us -> 0 us
  waiting for transfers between devices: 59.8 us -> 0 us
  starting transfers between devices: 52.4 us -> 0 us
  other arithmetic: 12.3 us -> 0 us
  matrix products: 4.54 us -> 0 us
  local copies, waits for them, and re-layouts: 7.88 us -> 4.4 us
    pallas_call x0 -> x1, Pallas kernels: none -> 91.3 us  [on_device(): pl.pallas_call(kernel, out_shape=(jax.ShapeDtypeStruct((piece, seqs), BF1...]
    all_to_all x2 -> x0, blocking collectives: 60.8 us -> none  [the longest x1 36.2 us: sent_and_summed(): lax.all_to_all(parts, axis, split_axis=0, concat_axis=0, tiled=True)]
    all_to_all x5 -> x0, waiting for transfers between devices: 59.8 us -> none  [the longest x2 34.7 us: sent_and_summed(): lax.all_to_all(parts, axis, split_axis=0, concat_axis=0, tiled=True)]
    all_to_all x5 -> x0, starting transfers between devices: 52.4 us -> none  [the longest x3 36.3 us: from_everyone(): lax.all_to_all(jnp.broadcast_to(array[None], (length, *array.shape)), axi...]
    dot_general x9 -> x0, matrix products: 4.54 us -> none  [the longest x6 3.3 us: partial_value(): return jnp.dot(scaled, weight, preferred_element_type=jnp.float32)]
    convert_element_type x10 -> x0, other arithmetic: 3.77 us -> none  [the longest x2 1.51 us: scaled_rows(): lax.dynamic_slice_in_dim(gain, block_first, block_cols).astype(jnp.float32)]
    reduce_sum x12 -> x0, other arithmetic: 3.72 us -> none  [the longest x1 2.33 us: delta_step(): readout = jnp.sum(new_state * queries[:, :, :, None], axis=2)]
    unnamed x23 -> x2, local copies, waits for them, and re-layouts: 0.98 us -> 4.4 us
  transfers between devices with their start and end apart: 5 -> 0, of which waited for: 5 -> 0; matrix products, arithmetic and copies ran while one was open for 4% -> 0% of each run, Pallas kernels for 0% -> 0%
where the time goes in v1:
time: 96.5 us; the launch traced here: 96.4 us
  Pallas kernels  91.3 us (95%)
  local copies, waits for them, and re-layouts  4.4 us (5%)
    pallas_call x1, Pallas kernels, on_device(): pl.pallas_call(kernel, out_shape=(jax.ShapeDtypeStruct((piece, seqs), BF1...  91.3 us
    unnamed x2, local copies, waits for them, and re-layouts  4.4 us

profile of v1, /device:TPU:33, one launch (start us, length us, event | category | flops | bytes accessed | tf_op | source)
XLA Modules:
  0.0 96.4 jit_solution(18111985738332249082)
XLA Ops:
  0.6 91.3 %layer.1 = (bf16[16,128]{1,0:T(8,128)(2,1)}, f32[8,4,128,128]{3,2,1,0:T(8,128)}) custom-call(bf16[16,128]{1,0:T(8,128)(2,1)} %bitcast.18, s32[8]{0:T(128)} %refs_1_.1, f32[8,4,128,128]{3,2,1,0:T(8,128)} %refs_2_.1, bf16[3,8,256]{2,1,0:T(8,128)(2,1)} %bitcast.15, bf16[3,8,256]{2,1,0:T(8,128)(2,1)} %bitcast.16, bf16[3,8,512]{2,1,0:T(8,128)(2,1)} %bitcast.14, ...), custom_call_target="tpu_custom_call" | custom-call | tf_op jit(solution)/shard_map/layer/pallas_call | solution.py:577
  92.0 1.3 %copy.27 = bf16[128,16]{0,1:T(8,128)(2,1)} copy(bf16[128,16]{0,1:T(8,128)(2,1)} %bitcast.17) | data formatting | bytes 8192
  93.3 3.1 %copy.28 = f32[8,4,128,128]{3,2,1,0:T(8,128)} copy(f32[8,4,128,128]{3,2,1,0:T(8,128)} %get-tuple-element.9) | data formatting | bytes 4194304

commit v2 on v1

--- a/solution.py
+++ b/solution.py
@@ -14,6 +14,12 @@
 MESH = pl.DeviceIdType.MESH
 F32 = jnp.float32
 BF16 = jnp.bfloat16
+
+PROJ = {7: 6, 8: 6, 4: 3, 5: 3}
+GATED = {}
+UP = {7: 6, 8: 6, 4: 3, 5: 3}
+HIDDEN = {6: 5, 7: 5, 8: 5}
+CHUNKS = 1
 
 class Inputs(typing.NamedTuple):
     stream: typing.Any
@@ -45,8 +51,8 @@
     return list(range(1, n // 2 + 1)) + [-o for o in range(1, (n + 1) // 2)]
 
 
-def tree(n, relayed):
-    return {o: (o - (1 if o > 0 else -1)) if abs(o) in relayed else 0 for o in ring_offsets(n)}
+def tree(n, relays):
+    return {o: relays.get(abs(o), 0) * (1 if o > 0 else -1) for o in ring_offsets(n)}
 
 
 def children_of(parents, o):
@@ -111,9 +117,9 @@
             total = total + self.recv[slot].astype(F32)
         return total
 
-    def leaves(self, relayed):
-        for o in sorted(self.parents, key=lambda o: -abs(o)):
-            if o not in self.inner and (self.parents[o] != 0) == relayed:
+    def leaves(self, among):
+        for o in sorted(among, key=lambda o: (self.parents.get(o, 0) == 0, -abs(o))):
+            if o != 0 and o not in self.inner:
                 self._send(o, self.part[o % self.x.n])
 
     def hubs(self):
@@ -136,12 +142,20 @@
     def begin(self):
         self._forward(0)
 
-    def finish(self):
-        order = sorted(self.parents, key=lambda o: (not children_of(self.parents, o), abs(o)))
-        for o in order:
+    def finish(self, among=None):
+        order = self.parents if among is None else [-o for o in among if o != 0]
+        for o in sorted(order, key=lambda o: (not children_of(self.parents, o), abs(o))):
             block = self.blocks.at[self.x.at(-o)]
             self.x.wait(o, block, block)
             self._forward(o)
+
+
+    @staticmethod
+    def finish_all(gathers):
+        parents = gathers[0].parents
+        for o in sorted(parents, key=lambda o: (not children_of(parents, o), abs(o))):
+            for gather in gathers:
+                gather.finish([-o])
 
 
 def rows_of(blocks):
@@ -184,13 +198,7 @@
         return Exchange("tp", n_tp, tp, *sems)
 
     x_stream = over_tp(r.stream_sems)
-    x_proj = over_kv(r.proj_sems)
-    barrier = pltpu.get_barrier_semaphore()
-    for o in range(1, n_tp):
-        pl.semaphore_signal(barrier, 1, device_id={"tp": x_stream.at(o)}, device_id_type=MESH)
-    for o in (1, -1):
-        pl.semaphore_signal(barrier, 1, device_id={"kv": x_proj.at(o)}, device_id_type=MESH)
-
+    x_proj = over_kv(r.proj_sems[0])
     started = []
 
     def load(source, into):
@@ -212,18 +220,15 @@
         conv_key=tp_cols(a.conv_key, key_cols),
         conv_value=tp_cols(a.conv_value, value_cols),
     )
-    first = Inputs(*range(len(a)))
-    order = [first.stream, first.norm_gain, first.w_decay, first.w_beta]
-    order += [first.w_query, first.w_key, first.w_value, first.w_gate]
-    order += [i for i in range(len(a)) if i not in order]
-    order.remove(first.delta_state)
-    order.append(first.delta_state)
-    copies = {i: load(sources[i], v[i]) for i in order}
-    c = Inputs(*[copies[i] for i in range(len(a))])
-
-    c.stream.wait()
     pieces = r.pieces
-    pieces[tp] = v.stream[...]
+    stream_copy = load(a.stream, pieces.at[tp])
+    barrier = pltpu.get_barrier_semaphore()
+    for o in range(1, n_tp):
+        pl.semaphore_signal(barrier, 1, device_id={"tp": x_stream.at(o)}, device_id_type=MESH)
+    for o in (1, -1):
+        pl.semaphore_signal(barrier, 1, device_id={"kv": x_proj.at(o)}, device_id_type=MESH)
+
+    stream_copy.wait()
     pl.semaphore_wait(barrier, n_tp - 1 + 2)
 
     def tell(step):
@@ -237,6 +242,18 @@
     g_stream = Gather(x_stream, {o: 0 for o in ring_offsets(n_tp)}, pieces)
     g_stream.begin()
     tell(1)
+    first = Inputs(*range(len(a)))
+    order = [first.norm_gain, first.w_decay, first.w_beta]
+    order += [first.w_query, first.w_key, first.w_value, first.w_gate]
+    order += [i for i in range(len(a)) if i not in order]
+    order.remove(first.stream)
+    order.remove(first.delta_state)
+    order.append(first.delta_state)
+    copies = {i: load(sources[i], v[i]) for i in order}
+    copies[first.stream] = stream_copy
+    c = Inputs(*[copies[i] for i in range(len(a))])
+    heard(1)
+    tell(2)
 
     def gain_row(copy, ref):
         copy.wait()
@@ -253,16 +270,17 @@
     for copy in (c.w_query, c.w_key, c.w_value, c.w_gate):
         copy.wait()
 
-    parents = d.scatter_tree
-    order = [0] + list(parents)
+    nearest = sorted([0] + ring_offsets(n_kv), key=lambda o: (abs(o), -o))
+    near, far = nearest[: n_kv // 2], nearest[n_kv // 2 :]
+    order = near + far
 
     def by_owner(values):
         r.rows[...] = values.reshape(n_kv, own, block)
         return jnp.concatenate([r.rows[x_proj.at(o)] for o in order], axis=0)
 
-    def put(part, at, product):
-        parts = product.reshape(n_kv, own, product.shape[1])
-        for i, o in enumerate(order):
+    def put(part, at, product, among):
+        parts = product.reshape(len(among), own, product.shape[1])
+        for i, o in enumerate(among):
             part[o % n_kv, :, at : at + product.shape[1]] = parts[i]
 
     def spread_squares(values):
@@ -271,26 +289,33 @@
 
     phase("stream")
     g_stream.finish()
+    heard(2)
+    tell(4)
     phase("project")
     stream_block = rows_of(pieces[...].astype(F32)).T
-    r.stream_block[...] = stream_block
     lhs = by_owner((stream_block * norm_row).astype(BF16).astype(F32)).astype(BF16)
-    at = 0
-    for weight in (v.w_query, v.w_key, v.w_value):
-        product = jnp.dot(lhs, weight[...], preferred_element_type=F32)
-        put(r.part_a, at, product)
-        at += product.shape[1]
-    rates = lax.dot_general(lhs, w_rates, (((1,), (1,)), ((), ())), preferred_element_type=F32)
-    lane = lax.broadcasted_iota(jnp.int32, rates.shape, 1)
-    put(r.part_a, at, jnp.where(lane < 2 * heads_all, rates, spread_squares(stream_block)))
-    s_proj = Scatter(x_proj, parents, r.part_a, r.send_a, r.recv_a)
-    s_proj.leaves(True)
-    heard(1)
-    tell(2)
-    put(r.part_g, 0, jnp.dot(lhs, v.w_gate[...], preferred_element_type=F32))
-    s_gate = Scatter(over_kv(r.gate_sems), parents, r.part_g, r.send_g, r.recv_g)
-    heard(2)
-    tell(4)
+    key_heads = key_cols // size
+    repeat = heads // key_heads
+    wide_v = repeat * size
+    s_proj = []
+    for g in range(key_heads):
+        part, at = r.part_a[g], 0
+        if g == 0:
+            rates = lax.dot_general(
+                lhs, w_rates, (((1,), (1,)), ((), ())), preferred_element_type=F32
+            )
+            lane = lax.broadcasted_iota(jnp.int32, rates.shape, 1)
+            rates = jnp.where(lane < 2 * heads_all, rates, spread_squares(stream_block))
+            put(part, 2 * size + 2 * wide_v, rates, order)
+        for weight, count in ((v.w_query, size), (v.w_key, size), (v.w_value, wide_v), (v.w_gate, wide_v)):
+            columns = weight[:, g * count : (g + 1) * count]
+            put(part, at, jnp.dot(lhs, columns, preferred_element_type=F32), order)
+            at += count
+        s_proj.append(
+            Scatter(over_kv(r.proj_sems[g]), d.proj_tree, part, r.send_a[g], r.recv_a[g])
+        )
+        s_proj[g].leaves([o for o in order if d.proj_tree.get(o, 0) != 0])
+    r.stream_rows[...] = by_owner(stream_block)
 
     phase("history")
     c.lengths.wait()
@@ -324,128 +349,150 @@
 
     heard(4)
     phase("hubs")
-    s_proj.leaves(False)
-    s_proj.hubs()
-    s_gate.leaves(True)
-    s_gate.leaves(False)
-    phase("gate_hubs")
-    s_gate.hubs()
+    direct = [o for o in order if d.proj_tree.get(o, 0) == 0]
+    for sums in s_proj:
+        sums.leaves(direct)
+    for sums in s_proj:
+        sums.hubs()
     for copy in (c.w_out, c.w_up, c.w_down, c.delta_state):
         copy.wait()
 
-    phase("sums")
-    sums = s_proj.total()
-    phase("delta")
-    at_v = 2 * key_cols
-    misc = sums[:, at_v + value_cols :]
-    scale = lax.rsqrt(misc[:, LANES - 1 : LANES] / width + EPSILON)
-    misc = misc * scale
-
-    def filtered(at, past, tap):
-        value = sums[:, at : at + past.shape[1]] * scale * tap + past
-        return value * jax.nn.sigmoid(value)
+    state = v.delta_state
 
     def unit(values):
         return values * lax.rsqrt(jnp.sum(values * values, axis=-1, keepdims=True) + EPSILON)
-
-    filtered_q = filtered(0, q_past, q_tap)
-    filtered_k = filtered(key_cols, k_past, k_tap)
-    values_now = filtered(at_v, v_past, v_tap)
-    fade_all = jnp.exp(-rate * softplus(misc[:, :heads_all] + bias))
-    strength_all = jax.nn.sigmoid(misc)
 
     def own_head(table, at):
         lanes = lax.broadcasted_iota(jnp.int32, table.shape, 1)
         one = jnp.sum(jnp.where(lanes == at, table, 0.0), axis=1, keepdims=True)
         return jnp.broadcast_to(one, (own, size))
 
-    key_heads = key_cols // size
-    repeat = heads // key_heads
-    state = v.delta_state
-    fades, strengths = [], []
-    for h in range(heads):
-        fades.append(jnp.where(lens == 1, 0.0, own_head(fade_all, tp * heads + h)))
-        strengths.append(own_head(strength_all, heads_all + tp * heads + h))
-    queries, keys, meets = [], [], []
+    out_copies, g_gated = [], []
     for g in range(key_heads):
-        queries.append(unit(filtered_q[:, g * size : (g + 1) * size]) * size ** (-0.5))
-        keys.append(unit(filtered_k[:, g * size : (g + 1) * size]))
-        meet = jnp.sum(queries[g] * keys[g], axis=1, keepdims=True)
-        meets.append(jnp.broadcast_to(meet, (own, size)))
-    out_copies = []
-    for s in range(own):
-        for g in range(key_heads):
-            key_wide = jnp.broadcast_to(keys[g][s : s + 1], (size, size)).T
-            query_wide = jnp.broadcast_to(queries[g][s : s + 1], (size, size)).T
-            for h in range(g * repeat, (g + 1) * repeat):
+        phase("sums")
+        sums = s_proj[g].total()
+        phase("delta")
+        if g == 0:
+            misc = sums[:, 2 * size + 2 * wide_v :]
+            scale = lax.rsqrt(misc[:, LANES - 1 : LANES] / width + EPSILON)
+            misc = misc * scale
+            fade_all = jnp.exp(-rate * softplus(misc[:, :heads_all] + bias))
+            strength_all = jax.nn.sigmoid(misc)
+
+        def filtered(at, past, tap, count):
+            ours = slice(g * count, (g + 1) * count)
+            value = sums[:, at : at + count] * scale * tap[:, ours] + past[:, ours]
+            return value * jax.nn.sigmoid(value)
+
+        query = unit(filtered(0, q_past, q_tap, size)) * size ** (-0.5)
+        key = unit(filtered(size, k_past, k_tap, size))
+        values_now = filtered(2 * size, v_past, v_tap, wide_v)
+        gate_in = sums[:, 2 * size + wide_v : 2 * size + 2 * wide_v] * scale
+        gate_in = gate_in * jax.nn.sigmoid(gate_in)
+        meet = jnp.sum(query * key, axis=1, keepdims=True)
+        ours = range(g * repeat, (g + 1) * repeat)
+        fades = [jnp.where(lens == 1, 0.0, own_head(fade_all, tp * heads + h)) for h in ours]
+        strengths = [own_head(strength_all, heads_all + tp * heads + h) for h in ours]
+        for s in range(own):
+            key_wide = jnp.broadcast_to(key[s : s + 1], (size, size)).T
+            query_wide = jnp.broadcast_to(query[s : s + 1], (size, size)).T
+            for i, h in enumerate(ours):
                 held = state[s, h]
-                fade = fades[h][s : s + 1]
-                value = values_now[s : s + 1, h * size : (h + 1) * size]
+                fade = fades[i][s : s + 1]
+                value = values_now[s : s + 1, i * size : (i + 1) * size]
                 recalled = fade * jnp.sum(held * key_wide, axis=0, keepdims=True)
-                update = strengths[h][s : s + 1] * (value - recalled)
+                update = strengths[i][s : s + 1] * (value - recalled)
                 read = fade * jnp.sum(held * query_wide, axis=0, keepdims=True)
-                r.readout[h, s : s + 1, :] = read + meets[g][s : s + 1] * update
+                r.readout[h, s : s + 1, :] = read + meet[s : s + 1] * update
                 state[s, h] = fade * held + key_wide * update
-        copy = pltpu.make_async_copy(state.at[s], new_state.at[s], r.out_sems.at[s])
+        gated = []
+        for i, h in enumerate(ours):
+            read = r.readout[h]
+            mean = jnp.mean(read * read, axis=1, keepdims=True)
+            gate = gate_in[:, i * size : (i + 1) * size]
+            gated.append(read * lax.rsqrt(mean + EPSILON) * gain_out * gate)
+        r.all_gated[g][kv] = jnp.concatenate(gated, axis=1).astype(BF16)
+        g_gated.append(Gather(over_kv(r.gated_sems[g]), d.gated_tree, r.all_gated[g]))
+        g_gated[g].begin()
+        heads_now = pl.ds(g * repeat, repeat)
+        copy = pltpu.make_async_copy(
+            state.at[:, heads_now], new_state.at[:, heads_now], r.out_sems.at[g]
+        )
         copy.start()
         out_copies.append(copy)
 
-    phase("gated")
-    gate_in = s_gate.total() * scale
-    gated = []
-    for h in range(heads):
-        read = r.readout[h]
-        mean = jnp.mean(read * read, axis=1, keepdims=True)
-        gate = gate_in[:, h * size : (h + 1) * size]
-        gate = gate * jax.nn.sigmoid(gate)
-        gated.append(read * lax.rsqrt(mean + EPSILON) * gain_out * gate)
-    r.all_gated[kv] = jnp.concatenate(gated, axis=1).astype(BF16)
-    g_gated = Gather(over_kv(r.gated_sems), d.gated_tree, r.all_gated)
-    g_gated.begin()
-    phase("gather_gated")
-    g_gated.finish()
-
-    phase("mixer")
-
-    def whole(blocks):
-        return rows_of(blocks[...].astype(F32)).astype(BF16)
-
-    mixer = jnp.dot(whole(r.all_gated), v.w_out[...], preferred_element_type=F32)
-    r.mixers[0] = mixer.astype(BF16)
-    x_mixer = over_tp(r.mixer_sems)
+    def rows_at(blocks, among):
+        parts = [blocks[x_proj.at(o)].astype(F32) for o in among]
+        return jnp.concatenate(parts, axis=0).astype(BF16)
+
     others = sorted(ring_offsets(n_tp), key=lambda o: -abs(o))
-    for o in others:
-        x_mixer.start(o, o, r.mixers.at[0], r.mixers.at[o % n_tp])
-    phase("sum_mixer")
-    for o in reversed(others):
-        x_mixer.wait(o, r.mixers.at[0], r.mixers.at[o % n_tp])
-        mixer = mixer + r.mixers[o % n_tp].astype(F32)
-    phase("up")
-    mixed = (r.stream_block[...] + mixer).astype(BF16).astype(F32)
-    r.mixed_turned[...] = mixed.T.reshape(n_tp, piece, seqs)
-
-    lhs = by_owner((mixed * mlp_row).astype(BF16).astype(F32)).astype(BF16)
-    put(r.part_u, 0, jnp.dot(lhs, v.w_up[...], preferred_element_type=F32))
-    put(r.part_u, ff, spread_squares(mixed))
-    s_up = Scatter(over_kv(r.up_sems), parents, r.part_u, r.send_u, r.recv_u)
-    s_up.leaves(True)
-    s_up.leaves(False)
+    halves = (near, far)
+    x_mixer, mixers = [], []
+    for i, among in enumerate(halves):
+        phase("gather_gated")
+        for gather in g_gated:
+            gather.finish(among)
+        phase("mixer")
+        mixer = 0.0
+        for g in range(key_heads):
+            weights = v.w_out[g * wide_v : (g + 1) * wide_v, :]
+            ours = rows_at(r.all_gated[g], among)
+            mixer = mixer + jnp.dot(ours, weights, preferred_element_type=F32)
+        mixers.append(mixer)
+        r.mixers[i][0] = mixer.astype(BF16)
+        x_mixer.append(over_tp(r.mixer_sems[i]))
+        for o in others:
+            x_mixer[i].start(o, o, r.mixers[i].at[0], r.mixers[i].at[o % n_tp])
+    s_up = [
+        Scatter(over_kv(r.up_sems[j]), d.up_tree, r.part_u[j], r.send_u[j], r.recv_u[j])
+        for j in range(CHUNKS)
+    ]
+    wide_u = ff // CHUNKS
+    at = 0
+    for i, among in enumerate(halves):
+        phase("sum_mixer")
+        mixer = mixers[i]
+        for o in reversed(others):
+            x_mixer[i].wait(o, r.mixers[i].at[0], r.mixers[i].at[o % n_tp])
+            mixer = mixer + r.mixers[i][o % n_tp].astype(F32)
+        phase("up")
+        count = own * len(among)
+        mixed = (r.stream_rows[at : at + count, :] + mixer).astype(BF16).astype(F32)
+        at += count
+        blocks = mixed.reshape(len(among), own, block)
+        for k, o in enumerate(among):
+            r.rows[x_proj.at(o)] = blocks[k]
+        lhs = (mixed * mlp_row).astype(BF16)
+        for j in range(CHUNKS):
+            weights = v.w_up[:, j * wide_u : (j + 1) * wide_u]
+            put(r.part_u[j], 0, jnp.dot(lhs, weights, preferred_element_type=F32), among)
+            s_up[j].leaves(among)
+    turned = rows_of(r.rows[...]).T
+    r.mixed_turned[...] = turned.reshape(n_tp, piece, seqs)
+    r.squares[kv] = jnp.sum(turned * turned, axis=0, keepdims=True)
+    g_squares = Gather(over_kv(r.square_sems), {o: 0 for o in ring_offsets(n_kv)}, r.squares)
     phase("up_hubs")
-    s_up.hubs()
-    phase("up_sums")
-    sums = s_up.total()
-    phase("hidden")
-    unit_scale = lax.rsqrt(sums[:, ff : ff + 1] / width + EPSILON)
-    raised = jnp.maximum(sums[:, :ff] * unit_scale, 0.0)
-    r.all_hidden[kv] = (raised * raised).astype(BF16)
-    g_hidden = Gather(over_kv(r.hidden_sems), d.hidden_tree, r.all_hidden)
-    g_hidden.begin()
+    for j in range(CHUNKS):
+        s_up[j].hubs()
+    g_squares.begin()
+    g_hidden = []
+    for j in range(CHUNKS):
+        phase("up_sums")
+        raised = jnp.maximum(s_up[j].total(), 0.0)
+        phase("hidden")
+        r.all_hidden[j][kv] = (raised * raised).astype(BF16)
+        g_hidden.append(Gather(over_kv(r.hidden_sems[j]), d.hidden_tree, r.all_hidden[j]))
+        g_hidden[j].begin()
     phase("gather_hidden")
-    g_hidden.finish()
+    Gather.finish_all(g_hidden)
     phase("down")
-    down = lax.dot_general(
-        v.w_down[...], whole(r.all_hidden), (((0,), (1,)), ((), ())), preferred_element_type=F32
-    )
+    down = 0.0
+    for j in range(CHUNKS):
+        hidden = rows_of(r.all_hidden[j][...].astype(F32)).astype(BF16)
+        weights = v.w_down[j * wide_u : (j + 1) * wide_u, :]
+        down = down + lax.dot_general(
+            weights, hidden, (((0,), (1,)), ((), ())), preferred_element_type=F32
+        )
     down = down.reshape(n_tp, piece, seqs)
     r.down_wide[...] = down
     r.downs[...] = down.astype(BF16)
@@ -453,16 +500,20 @@
     for o in others:
         x_down.start(o, o, r.downs.at[x_down.at(o)], r.arrived.at[o % n_tp])
     phase("sum_down")
+    g_squares.finish()
+    squares = jnp.sum(r.squares[...], axis=0)
+    unit_scale = lax.rsqrt(squares / width + EPSILON)
     total = r.down_wide[tp]
     for o in reversed(others):
         x_down.wait(o, r.downs.at[0], r.arrived.at[o % n_tp])
         total = total + r.arrived[o % n_tp].astype(F32)
     phase("leave")
-    r.result[...] = (r.mixed_turned[tp] + total).astype(BF16)
-    copy = pltpu.make_async_copy(r.result, result, r.out_sems.at[own])
+    r.result[...] = (r.mixed_turned[tp] + total * (unit_scale * unit_scale)).astype(BF16)
+    copy = pltpu.make_async_copy(r.result, result, r.out_sems.at[key_heads])
     copy.start()
     out_copies.append(copy)
-    exchanges = (x_stream, x_proj, s_gate.x, g_gated.x, x_mixer, s_up.x, g_hidden.x, x_down)
+    users = [*s_proj, *g_gated, *s_up, *g_hidden, g_squares]
+    exchanges = [x_stream, x_down, *x_mixer] + [user.x for user in users]
     for exchange in exchanges:
         exchange.drain()
     for copy in out_copies:
@@ -508,9 +559,10 @@
         piece=piece,
         taps=taps,
         heads_all=heads_all,
-        scatter_tree=tree(n_kv, (2, 4, 6, 8)),
-        gated_tree=tree(n_kv, ()),
-        hidden_tree=tree(n_kv, (2, 4, 6)),
+        proj_tree=tree(n_kv, PROJ),
+        up_tree=tree(n_kv, UP),
+        gated_tree=tree(n_kv, GATED),
+        hidden_tree=tree(n_kv, HIDDEN),
     )
     held = Inputs(*[pltpu.VMEM(x.shape, x.dtype) for x in given])
     held = held._replace(
@@ -521,8 +573,11 @@
         conv_key=pltpu.VMEM((taps, key_cols), BF16),
         conv_value=pltpu.VMEM((taps, value_cols), BF16),
     )
-    wide_a = 2 * key_cols + value_cols + LANES
-    wide_u = ff + LANES
+    key_heads = key_cols // size
+    wide_a = [2 * size + 2 * (value_cols // key_heads)] * key_heads
+    wide_a[0] += LANES
+    half = seqs // 2
+    chunks = range(CHUNKS)
 
     def sems(n):
         return (pltpu.SemaphoreType.DMA((n,)), pltpu.SemaphoreType.DMA((n,)))
@@ -535,33 +590,31 @@
 
     scratch = dict(
         stream_sems=sems(n_tp),
-        proj_sems=sems(n_kv),
-        gate_sems=sems(n_kv),
-        gated_sems=sems(n_kv),
-        mixer_sems=sems(n_tp),
-        up_sems=sems(n_kv),
-        hidden_sems=sems(n_kv),
+        proj_sems=[sems(n_kv) for _ in wide_a],
+        gated_sems=[sems(n_kv) for _ in wide_a],
+        mixer_sems=[sems(n_tp) for _ in range(2)],
+        up_sems=[sems(n_kv) for _ in chunks],
+        hidden_sems=[sems(n_kv) for _ in chunks],
         down_sems=sems(n_tp),
+        square_sems=sems(n_kv),
         load_sems=pltpu.SemaphoreType.DMA((len(given),)),
-        out_sems=pltpu.SemaphoreType.DMA((own + 1,)),
+        out_sems=pltpu.SemaphoreType.DMA((key_heads + 1,)),
         near_sems=pltpu.SemaphoreType.REGULAR((3,)),
         pieces=narrow(n_tp, piece, seqs),
         rows=wide(n_kv, own, block),
-        stream_block=wide(seqs, block),
-        part_a=wide(n_kv, own, wide_a),
-        send_a=narrow(n_kv, own, wide_a),
-        recv_a=narrow(n_kv, own, wide_a),
-        part_g=wide(n_kv, own, value_cols),
-        send_g=narrow(n_kv, own, value_cols),
-        recv_g=narrow(n_kv, own, value_cols),
+        stream_rows=wide(seqs, block),
+        part_a=[wide(n_kv, own, w) for w in wide_a],
+        send_a=[narrow(n_kv, own, w) for w in wide_a],
+        recv_a=[narrow(n_kv, own, w) for w in wide_a],
         readout=wide(heads, own, size),
-        all_gated=narrow(n_kv, own, value_cols),
-        mixers=narrow(n_tp, seqs, block),
+        all_gated=[narrow(n_kv, own, value_cols // key_heads) for _ in wide_a],
+        mixers=[narrow(n_tp, half, block) for _ in range(2)],
         mixed_turned=wide(n_tp, piece, seqs),
-        part_u=wide(n_kv, own, wide_u),
-        send_u=narrow(n_kv, own, wide_u),
-        recv_u=narrow(n_kv, own, wide_u),
-        all_hidden=narrow(n_kv, own, ff),
+        part_u=[wide(n_kv, own, ff // CHUNKS) for _ in chunks],
+        send_u=[narrow(n_kv, own, ff // CHUNKS) for _ in chunks],
+        recv_u=[narrow(n_kv, own, ff // CHUNKS) for _ in chunks],
+        squares=wide(n_kv, 1, seqs),
+        all_hidden=[narrow(n_kv, own, ff // CHUNKS) for _ in chunks],
         downs=narrow(n_tp, piece, seqs),
         down_wide=wide(n_tp, piece, seqs),
         arrived=narrow(n_tp, piece, seqs),
@@ -588,7 +641,37 @@
         ),
         name="layer",
     )(*given)
-    return (turned.T, new_state)
+    return finish(turned, new_state)
+
+
+def hand_on(turned, state, turned_out, state_out, turned_v, state_v, sems):
+    chunks = state.shape[0]
+    pairs = [(turned, turned_v, turned_out)]
+    pairs += [(state.at[i], state_v.at[i], state_out.at[i]) for i in range(chunks)]
+    reads = [pltpu.make_async_copy(p[0], p[1], sems.at[i]) for i, p in enumerate(pairs)]
+    writes = [pltpu.make_async_copy(p[1], p[2], sems.at[i + len(pairs)]) for i, p in enumerate(pairs)]
+    for copy in reads:
+        copy.start()
+    for read, write in zip(reads, writes):
+        read.wait()
+        write.start()
+    for copy in writes:
+        copy.wait()
+
+
+def finish(turned, state):
+    arrays = (turned, state)
+    turned, state = pl.pallas_call(
+        hand_on,
+        out_shape=[jax.ShapeDtypeStruct(x.shape, x.dtype) for x in arrays],
+        in_specs=[pl.BlockSpec(memory_space=pl.ANY)] * 2,
+        out_specs=[pl.BlockSpec(memory_space=pl.ANY)] * 2,
+        scratch_shapes=[pltpu.VMEM(x.shape, x.dtype) for x in arrays]
+        + [pltpu.SemaphoreType.DMA((2 + 2 * state.shape[0],))],
+        compiler_params=pltpu.CompilerParams(vmem_limit_bytes=67043328),
+        name="hand_on",
+    )(*arrays)
+    return (turned.T, state)
 
 
 def solution(mesh):

time: 96.5 us -> 86 us (0.89)
  Pallas kernels: 91.3 us -> 85.1 us
  local copies, waits for them, and re-layouts: 4.4 us -> 0 us
    pallas_call x1, Pallas kernels: 91.3 us -> 82.7 us  [on_device(): pl.pallas_call(kernel, out_shape=(jax.ShapeDtypeStruct((piece, seqs), BF1...]
    unnamed x2 -> x0, local copies, waits for them, and re-layouts: 4.4 us -> none
    pallas_call x0 -> x1, Pallas kernels: none -> 2.42 us  [finish(): pl.pallas_call(hand_on, out_shape=[jax.ShapeDtypeStruct(x.shape, x.dtype)...]
where the time goes in v2:
time: 86 us; the launch traced here: 85.8 us
  Pallas kernels  85.1 us (99%)
    pallas_call x1, Pallas kernels, on_device(): pl.pallas_call(kernel, out_shape=(jax.ShapeDtypeStruct((piece, seqs), BF1...  82.7 us
    pallas_call x1, Pallas kernels, finish(): pl.pallas_call(hand_on, out_shape=[jax.ShapeDtypeStruct(x.shape, x.dtype)...  2.42 us

profile of v2, /device:TPU:33, one launch (start us, length us, event | category | flops | bytes accessed | tf_op | source)
XLA Modules:
  0.0 85.8 jit_solution(14010530611475733770)
XLA Ops:
  0.6 82.7 %layer.1 = (bf16[16,128]{1,0:T(8,128)(2,1)}, f32[8,4,128,128]{3,2,1,0:T(8,128)}) custom-call(bf16[16,128]{1,0:T(8,128)(2,1)} %bitcast.17, s32[8]{0:T(128)} %refs_1_.1, f32[8,4,128,128]{3,2,1,0:T(8,128)} %refs_2_.1, bf16[3,8,256]{2,1,0:T(8,128)(2,1)} %bitcast.15, bf16[3,8,256]{2,1,0:T(8,128)(2,1)} %bitcast.16, bf16[3,8,512]{2,1,0:T(8,128)(2,1)} %bitcast.14, ...), custom_call_target="tpu_custom_call" | custom-call | tf_op jit(solution)/shard_map/layer/pallas_call | solution.py:630
  83.4 2.4 %hand_on.1 = (bf16[16,128]{1,0:T(8,128)(2,1)}, f32[8,4,128,128]{3,2,1,0:T(8,128)}) custom-call(bf16[16,128]{1,0:T(8,128)(2,1)} %get-tuple-element.6.turned, f32[8,4,128,128]{3,2,1,0:T(8,128)} %get-tuple-element.7.state), custom_call_target="tpu_custom_call" | custom-call | tf_op jit(solution)/shard_map/hand_on/pallas_call | solution.py:664
